TPU v7x, 512 devices: a 8x2x16 block of a 8x8x16 slice. The times are simulated.
512 devices in a mesh: grp: 2 (over y), sp: 32 (over z, core), tp: 8 (over x).
Axes of the slice: x: 8, y: 2, z: 16, core: 2. Of those that a mesh axis runs over, the one named last changes fastest.
The devices are a block of a 8x8x16 slice.
Arguments:
- glu_value: bfloat16 [8192, 2048], P(('grp', 'sp'), 'tp'), parts along dimension 0, may hold values from -6 to 6
- glu_gate: bfloat16 [8192, 2048], P(('grp', 'sp'), 'tp'), parts along dimension 0, may hold values from -9 to 9
- segments: int32 [8192], P(('grp', 'sp')), parts along dimension 0, may hold values from 0 to 7, never falling along the last dimension, each value on 1 to 2048 neighbouring positions
- conv_kernel: float32 [31, 2048], P(None, 'tp'), may hold values from -3.5 to 3.5
- norm_gain: float32 [2048], P('tp'), may hold values from 0.1 to 1.9
- norm_bias: float32 [2048], P('tp'), may hold values from -3 to 3
- residual: bfloat16 [8192, 2048], P(('grp', 'sp'), 'tp'), parts along dimension 0, may hold values from -6 to 6
- out_weight: bfloat16 [2048, 2048], P('tp'), may hold values from -0.125 to 0.125
- rms_gain: float32 [2048], replicated, may hold values from 0.1 to 1.9
- experts: int32 [8192, 4], P(('grp', 'sp')), parts along dimension 0, may hold values from 0 to 31, all different within a row; in each aligned block of 128 rows (0 to 127, 128 to 255, ...) at most 32 rows name the same one
- route_weights: float32 [8192, 4], P(('grp', 'sp')), parts along dimension 0, may hold values from 0.1 to 1
- glu_weight: bfloat16 [32, 2048, 2048], P('sp', None, 'tp'), may hold values from -0.5 to 0.5
- lin_weight: bfloat16 [32, 2048, 2048], P('sp', None, 'tp'), may hold values from -0.5 to 0.5
- down_weight: bfloat16 [32, 2048, 2048], P('sp', None, 'tp'), may hold values from -0.015625 to 0.015625
Outputs:
- layer_output: bfloat16 [8192, 2048], P(('grp', 'sp'), 'tp'), parts along dimension 0
There are 2 independent parts, one for each index of `grp`. A program takes and returns all parts, laid end to end along the dimension named above; an argument that names none is the same for every part. Nothing has to cross between parts.
Inputs may be any that keep to these rules, and one draw needn't show every extreme that they name: Each row names 4 different experts. In each aligned block of 128 rows no expert is named by more than 32 rows, and in some block an expert is named by exactly 32 rows. `segments`: never falling along positions; a document holds from 1 up to 2048 positions, and one holds exactly that many.
All inputs are finite; a program needn't handle non-finite values.
Results may differ from a plain program's by a relative error of at most 0.017.
Values may be sent and summed in bfloat16 or wider, within the bound.
No kernel may reach another device: no remote copies, remote signals or barrier semaphores. Data moves between devices by JAX's collectives and lax.ppermute only.
A program may use at most 64 MiB of HBM per device.

v0:
```python
import jax
import jax.numpy as jnp
from jax import lax
from jax.sharding import PartitionSpec as P

EPSILON = 1e-05
CLAMP_LIMIT = 7.0
SIGMOID_SCALE = 1.702


def passed_along(array, axis, by):
    length = lax.axis_size(axis)
    pairs = [(i, i + by) for i in range(length) if 0 <= i + by < length]
    return lax.ppermute(array, axis, pairs)


def copy_for_each(array, axis):
    copies = jnp.broadcast_to(array, (lax.axis_size(axis), *array.shape))
    return lax.all_to_all(copies, axis, split_axis=0, concat_axis=0, tiled=True)


def of_everyone(array, axis):
    return copy_for_each(array, axis).sum(axis=0)


def in_one(arrays, axis):
    ends = [0]
    for a in arrays:
        ends.append(ends[-1] + a.size)
    total = of_everyone(jnp.concatenate([a.ravel() for a in arrays]), axis)
    return tuple((total[b:e].reshape(a.shape) for a, b, e in zip(arrays, ends, ends[1:])))


def in_blocks(array, dim, length):
    lengths = array.shape
    blocks = array.reshape(*lengths[:dim], length, lengths[dim] // length, *lengths[dim + 1 :])
    return jnp.moveaxis(blocks, dim, 0)


def summed_on_arrival(array, axis, dim):
    length = lax.axis_size(axis)
    blocks = lax.all_to_all(in_blocks(array, dim, length), axis, 0, 0, tiled=True)
    return jnp.sum(blocks.astype(jnp.float32), axis=0)


def clamped_unit(gate_pre, lin_pre):
    gate_clip = jnp.minimum(gate_pre, CLAMP_LIMIT)
    linear = jnp.clip(lin_pre, -CLAMP_LIMIT, CLAMP_LIMIT)
    return gate_clip * jax.nn.sigmoid(SIGMOID_SCALE * gate_clip) * (linear + 1.0)


def shards(
    glu_value,
    glu_gate,
    segments,
    conv_kernel,
    norm_gain,
    norm_bias,
    residual,
    out_weight,
    rms_gain,
    experts,
    route_weights,
    glu_weight,
    lin_weight,
    down_weight,
):
    tok_count = glu_value.shape[0]
    local_width = glu_value.shape[1]
    model_width = out_weight.shape[1]
    kernel_reach = conv_kernel.shape[0] - 1
    top_count = experts.shape[1]
    local_experts = glu_weight.shape[0]
    sp_count = lax.axis_size("sp")
    expert_total = local_experts * sp_count
    capacity = min(tok_count, 2 * tok_count * top_count // expert_total)
    glu_out = (glu_value.astype(jnp.float32) * jax.nn.sigmoid(glu_gate.astype(jnp.float32))).astype(
        jnp.bfloat16
    )
    prev_rows, prev_segments = passed_along(
        (glu_out[tok_count - kernel_reach :], segments[tok_count - kernel_reach :]), "sp", 1
    )
    padded = jnp.concatenate([prev_rows, glu_out], axis=0).astype(jnp.float32)
    padded_segments = jnp.concatenate([prev_segments, segments], axis=0)
    conv_sum = jnp.zeros((tok_count, local_width), jnp.float32)
    for offset in range(kernel_reach + 1):
        lower = kernel_reach - offset
        window_rows = padded[lower : lower + tok_count]
        same_document = (padded_segments[lower : lower + tok_count] == segments).astype(jnp.float32)
        conv_sum = conv_sum + conv_kernel[offset][None, :] * window_rows * same_document[:, None]
    row_total, row_square = in_one(
        (jnp.sum(conv_sum, axis=1), jnp.sum(conv_sum * conv_sum, axis=1)), "tp"
    )
    row_mean = row_total / model_width
    row_var = row_square / model_width - row_mean * row_mean
    normed_conv = (conv_sum - row_mean[:, None]) * lax.rsqrt(row_var + EPSILON)[
        :, None
    ] * norm_gain + norm_bias
    swished = jax.nn.silu(normed_conv).astype(jnp.bfloat16)
    projected = jnp.dot(swished, out_weight, preferred_element_type=jnp.float32)
    conv_out = summed_on_arrival(projected.astype(jnp.bfloat16), "tp", 1)
    updated = (residual.astype(jnp.float32) + conv_out).astype(jnp.bfloat16)
    updated_float = updated.astype(jnp.float32)
    flat_experts = experts.reshape(-1)
    one_hot = (flat_experts[:, None] == jnp.arange(expert_total, dtype=jnp.int32)[None, :]).astype(
        jnp.int32
    )
    slot_rank = jnp.sum((jnp.cumsum(one_hot, axis=0) - 1) * one_hot, axis=1)
    slot_index = flat_experts * capacity + slot_rank
    token_order = jnp.arange(tok_count * top_count, dtype=jnp.int32) // top_count
    slot_token = (
        jnp.full((expert_total * capacity,), tok_count, jnp.int32).at[slot_index].set(token_order)
    )
    squares = of_everyone(jnp.sum(updated_float * updated_float, axis=1), "tp")
    width_start = lax.axis_index("tp") * local_width
    gain_cols = lax.dynamic_slice_in_dim(rms_gain, width_start, local_width)
    normed = (
        updated_float * lax.rsqrt(squares / model_width + EPSILON)[:, None] * gain_cols
    ).astype(jnp.bfloat16)
    normed_pad = jnp.concatenate([normed, jnp.zeros((1, local_width), jnp.bfloat16)], axis=0)
    packed = normed_pad[slot_token].reshape(sp_count, local_experts, capacity, local_width)
    portion = lax.all_gather(
        lax.all_to_all(packed, "sp", split_axis=0, concat_axis=0, tiled=True),
        "tp",
        axis=3,
        tiled=True,
    )
    gate_pre = jnp.einsum("slmd,ldf->slmf", portion, glu_weight, preferred_element_type=jnp.float32)
    lin_pre = jnp.einsum("slmd,ldf->slmf", portion, lin_weight, preferred_element_type=jnp.float32)
    hidden = clamped_unit(gate_pre, lin_pre).astype(jnp.bfloat16)
    summed = jnp.einsum(
        "slmf,lfd->slmd",
        lax.all_gather(hidden, "tp", axis=3, tiled=True),
        down_weight,
        preferred_element_type=jnp.float32,
    )
    results = summed.astype(jnp.bfloat16)
    returned = lax.all_to_all(results, "sp", split_axis=0, concat_axis=0, tiled=True)
    flat_back = returned.reshape(expert_total * capacity, local_width)
    picked = flat_back[slot_index].reshape(tok_count, top_count, local_width).astype(jnp.float32)
    routed_sum = jnp.sum(picked * route_weights[:, :, None], axis=1)
    return (updated_float + routed_sum).astype(jnp.bfloat16)


def solution(mesh):
    in_specs = (
        P(("grp", "sp"), "tp"),
        P(("grp", "sp"), "tp"),
        P(("grp", "sp")),
        P(None, "tp"),
        P("tp"),
        P("tp"),
        P(("grp", "sp"), "tp"),
        P("tp", None),
        P(),
        P(("grp", "sp"), None),
        P(("grp", "sp"), None),
        P("sp", None, "tp"),
        P("sp", None, "tp"),
        P("sp", None, "tp"),
    )
    out_specs = P(("grp", "sp"), "tp")
    return jax.shard_map(shards, mesh=mesh, in_specs=in_specs, out_specs=out_specs, check_vma=False)
```

profile of v0, /device:TPU:65, one launch (start us, length us, event | category | flops | bytes accessed | tf_op | source)
XLA Modules:
  0.0 342.0 jit_solution(18076324857074876872)
XLA Ops:
  6.6 0.8 slice.299
  7.4 7.0 %collective-permute-start.1 = (s32[30]{0:T(128)S(1)}, s32[30]{0:T(128)S(1)}, u32[]{:S(2)}, u32[]{:S(2)}) collective-permute-start(s32[30]{0:T(128)S(1)} %slice.299), channel_id=1, source_target_pairs={{0,8},{8,16},{16,24},{24,32},{32,40},{40,48},{48,56},{56,64},{64,7... | collective-permute-start | bytes 368 | tf_op jit(solution)/shard_map/ppermute | solution.py:14
  14.4 0.9 multiply_convert_fusion.1
  15.4 2.0 collective-permute-start
  17.3 1.0 fusion.117
  18.4 1.0 fusion.118
  19.3 31.4 %collective-permute-done.1 = s32[30]{0:T(128)S(1)} collective-permute-done((s32[30]{0:T(128)S(1)}, s32[30]{0:T(128)S(1)}, u32[]{:S(2)}, u32[]{:S(2)}) %collective-permute-start.1) | collective-permute-done | bytes 152 | tf_op jit(solution)/shard_map/ppermute | solution.py:14
  50.7 0.7 pad_add_fusion
  51.5 0.7 compare_convert_fusion.29
  52.2 0.7 compare_convert_fusion.28
  53.1 0.9 fusion.115
  54.6 3.5 %all-to-all-start = ((f32[8,1,256]{2,1,0:T(1,128)}), f32[8,1,256]{2,1,0:T(1,128)S(1)}, u32[]{:S(2)}, u32[]{:S(2)}) async-start(f32[8,1,256]{2,1,0:T(1,128)} %broadcast_in_dim.8), calls=%async_computation | async-start | bytes 16384 | tf_op jit(solution)/shard_map/all_to_all | solution.py:19
  58.5 6.0 %all-to-all-done = f32[8,1,256]{2,1,0:T(1,128)S(1)} async-done(((f32[8,1,256]{2,1,0:T(1,128)}), f32[8,1,256]{2,1,0:T(1,128)S(1)}, u32[]{:S(2)}, u32[]{:S(2)}) %all-to-all-start) | async-done | bytes 8224 | tf_op jit(solution)/shard_map/all_to_all | solution.py:19
  65.0 0.8 copy.57
  65.8 3.7 %all-to-all-start.1 = ((bf16[8,128,256]{2,1,0:T(8,128)(2,1)}), bf16[8,128,256]{2,1,0:T(8,128)(2,1)S(1)}, u32[]{:S(2)}, u32[]{:S(2)}) async-start(bf16[8,128,256]{2,1,0:T(8,128)(2,1)} %bitcast.123), calls=%async_computation.1 | async-start | bytes 1048576 | tf_op jit(solution)/shard_map/all_to_all | solution.py:42
  69.5 1.2 reduce-window.6
  71.3 2.4 scatter_custom_fusion
  73.8 7.1 %all-to-all-done.1 = bf16[8,128,256]{2,1,0:T(8,128)(2,1)S(1)} async-done(((bf16[8,128,256]{2,1,0:T(8,128)(2,1)}), bf16[8,128,256]{2,1,0:T(8,128)(2,1)S(1)}, u32[]{:S(2)}, u32[]{:S(2)}) %all-to-all-start.1) | async-done | bytes 524320 | tf_op jit(solution)/shard_map/all_to_all | solution.py:42
  81.7 4.3 %all-to-all-start.2 = ((f32[8,1,128]{2,1,0:T(1,128)}), f32[8,1,128]{2,1,0:T(1,128)S(1)}, u32[]{:S(2)}, u32[]{:S(2)}) async-start(f32[8,1,128]{2,1,0:T(1,128)} %broadcast_in_dim.9), calls=%async_computation.2 | async-start | bytes 8192 | tf_op jit(solution)/shard_map/all_to_all | solution.py:19
  86.0 0.8 dynamic_slice.3
  86.8 5.6 %all-to-all-done.2 = f32[8,1,128]{2,1,0:T(1,128)S(1)} async-done(((f32[8,1,128]{2,1,0:T(1,128)}), f32[8,1,128]{2,1,0:T(1,128)S(1)}, u32[]{:S(2)}, u32[]{:S(2)}) %all-to-all-start.2) | async-done | bytes 4128 | tf_op jit(solution)/shard_map/all_to_all | solution.py:19
  92.6 3.9 %gather_fusion = bf16[1024,256]{1,0:T(8,128)(2,1)S(1)} fusion(bf16[129,256]{1,0:T(8,128)(2,1)S(1)} %concatenate.15, s32[1024]{0:T(1024)S(1)} %fusion.108), kind=kCustom, calls=%fused_computation | custom fusion | bytes 1052672 | tf_op jit(solution)/shard_map/gather | solution.py:121
  96.5 53.6 %all_to_all.27 = bf16[32,1,32,256]{3,2,1,0:T(8,128)(2,1)} all-to-all(bf16[32,1,32,256]{3,2,1,0:T(8,128)(2,1)S(1)} %bitcast.127), channel_id=1, replica_groups=mesh['grp'=2,'sp'=32,'tp'=8] {'sp'}, dimensions={0} | all-to-all | bytes 1048576 | tf_op jit(solution)/shard_map/all_to_all | solution.py:123
  150.2 54.3 %all-gather.3.cloned.1.call-done = bf16[32,1,32,2048]{3,2,0,1:T(8,128)(2,1)} async-done(((bf16[32,1,32,256]{3,2,0,1:T(8,128)(2,1)}), bf16[32,1,32,2048]{3,2,0,1:T(8,128)(2,1)}) %all-gather.3.cloned.1.call-update) | async-done | bytes 4194320 | tf_op jit(solution)/shard_map/all_gather | solution.py:122
  204.5 3.6 %fusion.9 = f32[32,1,32,256]{3,2,0,1:T(8,128)S(1)} fusion(bf16[32,1,32,2048]{3,2,0,1:T(8,128)(2,1)} %all-gather.3.cloned.1.call-done, bf16[1,2048,256]{2,1,0:T(8,128)(2,1)S(1)} %copy-done.7), kind=kOutput, calls=%fused_computation.11 | convolution fusion | flops 1074003968 | bytes 6291456 | tf_op jit(solution)/shard_map/slmd,ldf->slmf/dot_general | solution.py:128
  208.1 3.5 %fusion.24 = bf16[32,1,32,256]{3,2,0,1:T(8,128)(2,1)} fusion(bf16[32,1,32,2048]{3,2,0,1:T(8,128)(2,1)S(1)} %copy-done.6, bf16[1,2048,256]{2,1,0:T(8,128)(2,1)} %param.26, f32[32,1,32,256]{3,2,0,1:T(8,128)S(1)} %fusion.9), kind=kOutput, calls=%fused_computation.16 | convolution fusion | flops 1076101120 | bytes 6815744 | tf_op jit(solution)/shard_map/slmd,ldf->slmf/dot_general | solution.py:129
  211.7 67.7 %all-gather.5.cloned.1.call-done = bf16[32,1,32,2048]{3,2,0,1:T(8,128)(2,1)} async-done(((bf16[32,1,32,256]{3,2,0,1:T(8,128)(2,1)}), bf16[32,1,32,2048]{3,2,0,1:T(8,128)(2,1)}) %all-gather.5.cloned.1.call-update) | async-done | bytes 4194320 | tf_op jit(solution)/shard_map/all_gather | solution.py:133
  279.4 4.2 %fusion.30 = bf16[32,1,32,256]{3,2,1,0:T(8,128)(2,1)} fusion(bf16[32,1,32,2048]{3,2,0,1:T(8,128)(2,1)} %all-gather.5.cloned.1.call-done, bf16[1,2048,256]{2,1,0:T(8,128)(2,1)S(1)} %copy-done.8), kind=kOutput, calls=%fused_computation.18 | convolution fusion | flops 1074003968 | bytes 5767168 | tf_op jit(solution)/shard_map/slmf,lfd->slmd/dot_general | solution.py:131
  283.6 15.1 %all-to-all-start.4 = ((bf16[32,1,32,256]{3,2,1,0:T(8,128)(2,1)}), bf16[32,1,32,256]{3,2,1,0:T(8,128)(2,1)S(1)}, u32[]{:S(2)}, u32[]{:S(2)}) async-start(bf16[32,1,32,256]{3,2,1,0:T(8,128)(2,1)} %fusion.30), calls=%async_computation.4 | async-start | bytes 1048576 | tf_op jit(solution)/shard_map/all_to_all | solution.py:138
  298.8 33.2 %all-to-all-done.4 = bf16[32,1,32,256]{3,2,1,0:T(8,128)(2,1)S(1)} async-done(((bf16[32,1,32,256]{3,2,1,0:T(8,128)(2,1)}), bf16[32,1,32,256]{3,2,1,0:T(8,128)(2,1)S(1)}, u32[]{:S(2)}, u32[]{:S(2)}) %all-to-all-start.4) | async-done | bytes 524320 | tf_op jit(solution)/shard_map/all_to_all | solution.py:138
  332.0 1.9 gather_fusion.1
  334.5 0.6 fusion.39
  (55 shorter events, 3.9 us)
Async XLA Ops:
  6.5 58.0 %copy-start = (bf16[256,2048]{1,0:T(8,128)(2,1)S(1)}, bf16[256,2048]{1,0:T(8,128)(2,1)}, u32[]{:S(2)}) copy-start(bf16[256,2048]{1,0:T(8,128)(2,1)} %param.21) | copy-start | bytes 3145732
  6.6 51.6 %copy-start.2 = (s32[128,4]{0,1:T(4,128)S(1)}, s32[128,4]{0,1:T(4,128)}, u32[]{:S(2)}) copy-start(s32[128,4]{0,1:T(4,128)} %param.23) | copy-start | bytes 6148
  6.6 58.0 %copy-start.5 = (f32[256]{0:T(256)S(1)}, f32[256]{0:T(256)}, u32[]{:S(2)}) copy-start(f32[256]{0:T(256)} %param.18) | copy-start | bytes 3076
  6.6 58.0 %copy-start.4 = (f32[256]{0:T(256)S(1)}, f32[256]{0:T(256)}, u32[]{:S(2)}) copy-start(f32[256]{0:T(256)} %param.19) | copy-start | bytes 3076
  7.4 43.4 %collective-permute-start.1 = (s32[30]{0:T(128)S(1)}, s32[30]{0:T(128)S(1)}, u32[]{:S(2)}, u32[]{:S(2)}) collective-permute-start(s32[30]{0:T(128)S(1)} %slice.299), channel_id=1, source_target_pairs={{0,8},{8,16},{16,24},{24,32},{32,40},{40,48},{48,56},{56,64},{64,7... | collective-permute-start | bytes 368 | tf_op jit(solution)/shard_map/ppermute | solution.py:14
  15.4 37.6 %collective-permute-start = (bf16[30,256]{1,0:T(8,128)(2,1)S(1)}, bf16[30,256]{1,0:T(8,128)(2,1)S(1)}, u32[]{:S(2)}, u32[]{:S(2)}) collective-permute-start(bf16[30,256]{1,0:T(8,128)(2,1)S(1)} %slice.396), channel_id=1, source_target_pairs={{0,8},{8,16},{16,24},{24,32},{32,40},{40,48},{48,56},{56,64},{64,7... | collective-permute-start | bytes 46088 | tf_op jit(solution)/shard_map/ppermute | solution.py:14
  53.0 27.9 %copy-start.1 = (bf16[128,256]{1,0:T(8,128)(2,1)S(1)}, bf16[128,256]{1,0:T(8,128)(2,1)}, u32[]{:S(2)}) copy-start(bf16[128,256]{1,0:T(8,128)(2,1)} %param.20) | copy-start | bytes 196612
  54.6 9.9 %all-to-all-start = ((f32[8,1,256]{2,1,0:T(1,128)}), f32[8,1,256]{2,1,0:T(1,128)S(1)}, u32[]{:S(2)}, u32[]{:S(2)}) async-start(f32[8,1,256]{2,1,0:T(1,128)} %broadcast_in_dim.8), calls=%async_computation | async-start | bytes 16384 | tf_op jit(solution)/shard_map/all_to_all | solution.py:19
  65.8 15.1 %all-to-all-start.1 = ((bf16[8,128,256]{2,1,0:T(8,128)(2,1)}), bf16[8,128,256]{2,1,0:T(8,128)(2,1)S(1)}, u32[]{:S(2)}, u32[]{:S(2)}) async-start(bf16[8,128,256]{2,1,0:T(8,128)(2,1)} %bitcast.123), calls=%async_computation.1 | async-start | bytes 1048576 | tf_op jit(solution)/shard_map/all_to_all | solution.py:42
  69.5 135.0 %copy-start.7 = (bf16[1,2048,256]{2,1,0:T(8,128)(2,1)S(1)}, bf16[1,2048,256]{2,1,0:T(8,128)(2,1)}, u32[]{:S(2)}) copy-start(bf16[1,2048,256]{2,1,0:T(8,128)(2,1)} %param.25) | copy-start | bytes 3145732
  81.7 10.8 %all-to-all-start.2 = ((f32[8,1,128]{2,1,0:T(1,128)}), f32[8,1,128]{2,1,0:T(1,128)S(1)}, u32[]{:S(2)}, u32[]{:S(2)}) async-start(f32[8,1,128]{2,1,0:T(1,128)} %broadcast_in_dim.9), calls=%async_computation.2 | async-start | bytes 8192 | tf_op jit(solution)/shard_map/all_to_all | solution.py:19
  86.0 118.6 %all-gather.3.cloned.1.call-start = ((), (), s32[]{:S(2)}) async-start(), calls=%async_computation.5 | async-start | bytes 4718592 | tf_op jit(solution)/shard_map/all_gather | solution.py:122
  150.2 129.2 %all-gather.5.cloned.1.call-start = ((), (), s32[]{:S(2)}) async-start(), calls=%async_computation.6 | async-start | bytes 4718592 | tf_op jit(solution)/shard_map/all_gather | solution.py:133
  204.5 3.6 %copy-start.6 = (bf16[32,1,32,2048]{3,2,0,1:T(8,128)(2,1)S(1)}, bf16[32,1,32,2048]{3,2,0,1:T(8,128)(2,1)}, u32[]{:S(2)}) copy-start(bf16[32,1,32,2048]{3,2,0,1:T(8,128)(2,1)} %all-gather.3.cloned.1.call-done) | copy-start | bytes 12582916
  208.1 71.2 %copy-start.8 = (bf16[1,2048,256]{2,1,0:T(8,128)(2,1)S(1)}, bf16[1,2048,256]{2,1,0:T(8,128)(2,1)}, u32[]{:S(2)}) copy-start(bf16[1,2048,256]{2,1,0:T(8,128)(2,1)} %param.27) | copy-start | bytes 3145732
  211.7 87.0 %copy-start.3 = (f32[128,4]{0,1:T(4,128)S(1)}, f32[128,4]{0,1:T(4,128)}, u32[]{:S(2)}) copy-start(f32[128,4]{0,1:T(4,128)} %param.24) | copy-start | bytes 6148
  283.6 48.4 %all-to-all-start.4 = ((bf16[32,1,32,256]{3,2,1,0:T(8,128)(2,1)}), bf16[32,1,32,256]{3,2,1,0:T(8,128)(2,1)S(1)}, u32[]{:S(2)}, u32[]{:S(2)}) async-start(bf16[32,1,32,256]{3,2,1,0:T(8,128)(2,1)} %fusion.30), calls=%async_computation.4 | async-start | bytes 1048576 | tf_op jit(solution)/shard_map/all_to_all | solution.py:138
Sparse Core Ops, SparseCore 0:
  150.3 54.1 all-gather.2
  211.8 67.5 all-gather.4
where the time goes:
time: 343 us; the launch traced here: 342 us
  waiting for transfers between devices  205 us (60%)
  blocking collectives  53.6 us (16%)
  starting transfers between devices  35.7 us (10%)
  local copies, waits for them, and re-layouts  15 us (4%)
  between operations  13.7 us (4%)
  matrix products  11.7 us (3%)
  other arithmetic  6.8 us (2%)
    all_gather x1, waiting for transfers between devices, shards(): lax.all_gather(hidden, 'tp', axis=3, tiled=True)  67.7 us
    all_gather x1, waiting for transfers between devices, shards(): lax.all_gather(lax.all_to_all(packed, 'sp', split_axis=0, concat_axis=0,...  54.3 us
    all_to_all x1, blocking collectives, shards(): lax.all_to_all(packed, 'sp', split_axis=0, concat_axis=0, tiled=True)  53.6 us
    all_to_all x1, waiting for transfers between devices, shards(): lax.all_to_all(results, 'sp', split_axis=0, concat_axis=0, tiled=True)  33.2 us
    ppermute x2, waiting for transfers between devices, passed_along(): return lax.ppermute(array, axis, pairs)  31.5 us
    all_to_all x1, starting transfers between devices, shards(): lax.all_to_all(results, 'sp', split_axis=0, concat_axis=0, tiled=True)  15.1 us
    all_to_all x2, waiting for transfers between devices, copy_for_each(): return lax.all_to_all(copies, axis, split_axis=0, concat_axis=0, tiled=True)  11.7 us
    ppermute x2, starting transfers between devices, passed_along(): return lax.ppermute(array, axis, pairs)  9 us
  transfers between devices with their start and end apart: 8, of which 7 were waited for; matrix products, arithmetic and copies ran while one was open for 3% of the time, Pallas kernels for 0%

commit v1 on v0

--- a/solution.py
+++ b/solution.py
@@ -130,7 +130,9 @@
     hidden = clamped_unit(gate_pre, lin_pre).astype(jnp.bfloat16)
     summed = jnp.einsum(
         "slmf,lfd->slmd",
-        lax.all_gather(hidden, "tp", axis=3, tiled=True),
+        jnp.concatenate(
+            lax.all_to_all(jnp.stack([hidden] * lax.axis_size("tp")), "tp", 0, 0), axis=3
+        ),
         down_weight,
         preferred_element_type=jnp.float32,
     )

time: 343 us -> 383 us (1.12)
  blocking collectives: 53.6 us -> 146 us
  waiting for transfers between devices: 205 us -> 138 us
  local copies, waits for them, and re-layouts: 15 us -> 29.4 us
    all_to_all x0 -> x1, blocking collectives: none -> 92.8 us  [shards(): lax.all_to_all(jnp.stack([hidden] * lax.axis_size('tp')), 'tp', 0, 0)]
    all_gather x1 -> x0, waiting for transfers between devices: 67.7 us -> none  [shards(): lax.all_gather(hidden, 'tp', axis=3, tiled=True)]
    another operation x1 -> x3, local copies, waits for them, and re-layouts: 0.01 us -> 8.03 us
    reshape x0 -> x1, local copies, waits for them, and re-layouts: none -> 6.25 us  [shards(): jnp.concatenate(lax.all_to_all(jnp.stack([hidden] * lax.axis_size('tp')),...]
  transfers between devices with their start and end apart: 8 -> 7, of which waited for: 7 -> 6; matrix products, arithmetic and copies ran while one was open for 3% -> 3% of each run, Pallas kernels for 0% -> 0%
where the time goes in v1:
time: 383 us; the launch traced here: 382 us
  blocking collectives  146 us (38%)
  waiting for transfers between devices  138 us (36%)
  starting transfers between devices  38.6 us (10%)
  local copies, waits for them, and re-layouts  29.4 us (8%)
  between operations  13.7 us (4%)
  matrix products  9.6 us (3%)
  other arithmetic  6.8 us (2%)
    all_to_all x1, blocking collectives, shards(): lax.all_to_all(jnp.stack([hidden] * lax.axis_size('tp')), 'tp', 0, 0)  92.8 us
    all_gather x1, waiting for transfers between devices, shards(): lax.all_gather(lax.all_to_all(packed, 'sp', split_axis=0, concat_axis=0,...  54.4 us
    all_to_all x1, blocking collectives, shards(): lax.all_to_all(packed, 'sp', split_axis=0, concat_axis=0, tiled=True)  53.6 us
    all_to_all x1, waiting for transfers between devices, shards(): lax.all_to_all(results, 'sp', split_axis=0, concat_axis=0, tiled=True)  33.2 us
    ppermute x2, waiting for transfers between devices, passed_along(): return lax.ppermute(array, axis, pairs)  31.5 us
    all_to_all x1, starting transfers between devices, shards(): lax.all_to_all(results, 'sp', split_axis=0, concat_axis=0, tiled=True)  18 us
    all_to_all x2, waiting for transfers between devices, copy_for_each(): return lax.all_to_all(copies, axis, split_axis=0, concat_axis=0, tiled=True)  11.7 us
    ppermute x2, starting transfers between devices, passed_along(): return lax.ppermute(array, axis, pairs)  9 us
  transfers between devices with their start and end apart: 7, of which 6 were waited for; matrix products, arithmetic and copies ran while one was open for 3% of the time, Pallas kernels for 0%

profile of v1, /device:TPU:65, one launch (start us, length us, event | category | flops | bytes accessed | tf_op | source)
XLA Modules:
  0.0 382.2 jit_solution(6141006946376987191)
XLA Ops:
  6.6 0.8 slice.299
  7.4 7.0 %collective-permute-start.1 = (s32[30]{0:T(128)S(1)}, s32[30]{0:T(128)S(1)}, u32[]{:S(2)}, u32[]{:S(2)}) collective-permute-start(s32[30]{0:T(128)S(1)} %slice.299), channel_id=1, source_target_pairs={{0,8},{8,16},{16,24},{24,32},{32,40},{40,48},{48,56},{56,64},{64,7... | collective-permute-start | bytes 368 | tf_op jit(solution)/shard_map/ppermute | solution.py:14
  14.4 0.9 multiply_convert_fusion.1
  15.4 2.0 collective-permute-start
  17.3 1.0 fusion.113
  18.4 1.0 fusion.114
  19.3 31.4 %collective-permute-done.1 = s32[30]{0:T(128)S(1)} collective-permute-done((s32[30]{0:T(128)S(1)}, s32[30]{0:T(128)S(1)}, u32[]{:S(2)}, u32[]{:S(2)}) %collective-permute-start.1) | collective-permute-done | bytes 152 | tf_op jit(solution)/shard_map/ppermute | solution.py:14
  51.5 0.7 compare_convert_fusion.29
  52.2 0.7 compare_convert_fusion.28
  53.1 0.9 fusion.111
  54.6 3.5 all-to-all-start
  58.5 6.0 %all-to-all-done = f32[8,1,256]{2,1,0:T(1,128)S(1)} async-done(((f32[8,1,256]{2,1,0:T(1,128)}), f32[8,1,256]{2,1,0:T(1,128)S(1)}, u32[]{:S(2)}, u32[]{:S(2)}) %all-to-all-start) | async-done | bytes 8224 | tf_op jit(solution)/shard_map/all_to_all | solution.py:19
  65.0 0.8 copy.60
  65.8 3.7 all-to-all-start.1
  69.5 1.2 reduce-window.6
  71.3 2.4 scatter_custom_fusion
  73.8 7.1 %all-to-all-done.1 = bf16[8,128,256]{2,1,0:T(8,128)(2,1)S(1)} async-done(((bf16[8,128,256]{2,1,0:T(8,128)(2,1)}), bf16[8,128,256]{2,1,0:T(8,128)(2,1)S(1)}, u32[]{:S(2)}, u32[]{:S(2)}) %all-to-all-start.1) | async-done | bytes 524320 | tf_op jit(solution)/shard_map/all_to_all | solution.py:42
  81.7 4.3 %all-to-all-start.2 = ((f32[8,1,128]{2,1,0:T(1,128)}), f32[8,1,128]{2,1,0:T(1,128)S(1)}, u32[]{:S(2)}, u32[]{:S(2)}) async-start(f32[8,1,128]{2,1,0:T(1,128)} %broadcast_in_dim.9), calls=%async_computation.2 | async-start | bytes 8192 | tf_op jit(solution)/shard_map/all_to_all | solution.py:19
  86.0 0.8 dynamic_slice.3
  86.8 5.6 %all-to-all-done.2 = f32[8,1,128]{2,1,0:T(1,128)S(1)} async-done(((f32[8,1,128]{2,1,0:T(1,128)}), f32[8,1,128]{2,1,0:T(1,128)S(1)}, u32[]{:S(2)}, u32[]{:S(2)}) %all-to-all-start.2) | async-done | bytes 4128 | tf_op jit(solution)/shard_map/all_to_all | solution.py:19
  92.6 3.9 %gather_fusion = bf16[1024,256]{1,0:T(8,128)(2,1)S(1)} fusion(bf16[129,256]{1,0:T(8,128)(2,1)S(1)} %concatenate.15, s32[1024]{0:T(1024)S(1)} %fusion.104), kind=kCustom, calls=%fused_computation | custom fusion | bytes 1052672 | tf_op jit(solution)/shard_map/gather | solution.py:121
  96.5 53.6 %all_to_all.32 = bf16[32,1,32,256]{3,2,1,0:T(8,128)(2,1)} all-to-all(bf16[32,1,32,256]{3,2,1,0:T(8,128)(2,1)S(1)} %bitcast.133), channel_id=1, replica_groups=mesh['grp'=2,'sp'=32,'tp'=8] {'sp'}, dimensions={0} | all-to-all | bytes 1048576 | tf_op jit(solution)/shard_map/all_to_all | solution.py:123
  150.2 54.4 %all-gather.2.cloned.1.call-done = bf16[32,1,32,2048]{3,2,0,1:T(8,128)(2,1)} async-done(((bf16[32,1,32,256]{3,2,0,1:T(8,128)(2,1)}), bf16[32,1,32,2048]{3,2,0,1:T(8,128)(2,1)}) %all-gather.2.cloned.1.call-update) | async-done | bytes 4194320 | tf_op jit(solution)/shard_map/all_gather | solution.py:122
  204.5 3.6 fusion.7
  208.3 1.4 fusion.26
  210.2 92.8 %all_to_all.33 = bf16[8,32,1,32,256]{4,3,1,2,0:T(8,128)(2,1)S(1)} all-to-all(bf16[8,32,1,32,256]{4,3,1,2,0:T(8,128)(2,1)S(1)} %stack.2), channel_id=1, replica_groups=mesh['grp'=2,'sp'=32,'tp'=8] {'tp'}, dimensions={0} | all-to-all | bytes 8388608 | tf_op jit(solution)/shard_map/all_to_all | solution.py:134
  303.0 6.3 %copy.50 = bf16[32,1,32,8,256]{4,3,2,0,1:T(8,128)(2,1)} copy(bf16[32,1,32,8,256]{4,2,0,1,3:T(8,128)(2,1)S(1)} %bitcast.129) | data formatting | bytes 8388608 | tf_op jit(solution)/shard_map/reshape | solution.py:133
  309.2 7.5 %reshape.151 = bf16[32,32,2048]{2,1,0:T(8,128)(2,1)} reshape(bf16[32,1,32,8,256]{4,3,2,0,1:T(8,128)(2,1)} %copy.50) | data formatting | bytes 8388608 | tf_op jit(solution)/shard_map/reshape.18
  316.7 4.2 %fusion.25 = bf16[32,1,32,256]{3,2,1,0:T(8,128)(2,1)} fusion(bf16[32,32,2048]{2,1,0:T(8,128)(2,1)} %reshape.151, bf16[1,2048,256]{2,1,0:T(8,128)(2,1)S(1)} %copy-done.9), kind=kOutput, calls=%fused_computation.16 | convolution fusion | flops 1074003968 | bytes 5767168 | tf_op jit(solution)/shard_map/slmf,lfd->slmd/dot_general | solution.py:131
  321.0 18.0 %all-to-all-start.5 = ((bf16[32,1,32,256]{3,2,1,0:T(8,128)(2,1)}), bf16[32,1,32,256]{3,2,1,0:T(8,128)(2,1)S(1)}, u32[]{:S(2)}, u32[]{:S(2)}) async-start(bf16[32,1,32,256]{3,2,1,0:T(8,128)(2,1)} %fusion.25), calls=%async_computation.5 | async-start | bytes 1048576 | tf_op jit(solution)/shard_map/all_to_all | solution.py:140
  339.1 33.2 %all-to-all-done.5 = bf16[32,1,32,256]{3,2,1,0:T(8,128)(2,1)S(1)} async-done(((bf16[32,1,32,256]{3,2,1,0:T(8,128)(2,1)}), bf16[32,1,32,256]{3,2,1,0:T(8,128)(2,1)S(1)}, u32[]{:S(2)}, u32[]{:S(2)}) %all-to-all-start.5) | async-done | bytes 524320 | tf_op jit(solution)/shard_map/all_to_all | solution.py:140
  372.3 1.9 gather_fusion.1
  (58 shorter events, 5.8 us)
Async XLA Ops:
  6.5 58.0 %copy-start = (bf16[256,2048]{1,0:T(8,128)(2,1)S(1)}, bf16[256,2048]{1,0:T(8,128)(2,1)}, u32[]{:S(2)}) copy-start(bf16[256,2048]{1,0:T(8,128)(2,1)} %param.21) | copy-start | bytes 3145732
  6.6 51.6 %copy-start.2 = (s32[128,4]{0,1:T(4,128)S(1)}, s32[128,4]{0,1:T(4,128)}, u32[]{:S(2)}) copy-start(s32[128,4]{0,1:T(4,128)} %param.23) | copy-start | bytes 6148
  6.6 58.0 %copy-start.5 = (f32[256]{0:T(256)S(1)}, f32[256]{0:T(256)}, u32[]{:S(2)}) copy-start(f32[256]{0:T(256)} %param.18) | copy-start | bytes 3076
  6.6 58.0 %copy-start.4 = (f32[256]{0:T(256)S(1)}, f32[256]{0:T(256)}, u32[]{:S(2)}) copy-start(f32[256]{0:T(256)} %param.19) | copy-start | bytes 3076
  7.4 43.4 %collective-permute-start.1 = (s32[30]{0:T(128)S(1)}, s32[30]{0:T(128)S(1)}, u32[]{:S(2)}, u32[]{:S(2)}) collective-permute-start(s32[30]{0:T(128)S(1)} %slice.299), channel_id=1, source_target_pairs={{0,8},{8,16},{16,24},{24,32},{32,40},{40,48},{48,56},{56,64},{64,7... | collective-permute-start | bytes 368 | tf_op jit(solution)/shard_map/ppermute | solution.py:14
  15.4 37.6 %collective-permute-start = (bf16[30,256]{1,0:T(8,128)(2,1)S(1)}, bf16[30,256]{1,0:T(8,128)(2,1)S(1)}, u32[]{:S(2)}, u32[]{:S(2)}) collective-permute-start(bf16[30,256]{1,0:T(8,128)(2,1)S(1)} %slice.396), channel_id=1, source_target_pairs={{0,8},{8,16},{16,24},{24,32},{32,40},{40,48},{48,56},{56,64},{64,7... | collective-permute-start | bytes 46088 | tf_op jit(solution)/shard_map/ppermute | solution.py:14
  53.0 27.9 %copy-start.1 = (bf16[128,256]{1,0:T(8,128)(2,1)S(1)}, bf16[128,256]{1,0:T(8,128)(2,1)}, u32[]{:S(2)}) copy-start(bf16[128,256]{1,0:T(8,128)(2,1)} %param.20) | copy-start | bytes 196612
  54.6 9.9 %all-to-all-start = ((f32[8,1,256]{2,1,0:T(1,128)}), f32[8,1,256]{2,1,0:T(1,128)S(1)}, u32[]{:S(2)}, u32[]{:S(2)}) async-start(f32[8,1,256]{2,1,0:T(1,128)} %broadcast_in_dim.8), calls=%async_computation | async-start | bytes 16384 | tf_op jit(solution)/shard_map/all_to_all | solution.py:19
  65.8 15.1 %all-to-all-start.1 = ((bf16[8,128,256]{2,1,0:T(8,128)(2,1)}), bf16[8,128,256]{2,1,0:T(8,128)(2,1)S(1)}, u32[]{:S(2)}, u32[]{:S(2)}) async-start(bf16[8,128,256]{2,1,0:T(8,128)(2,1)} %bitcast.128), calls=%async_computation.1 | async-start | bytes 1048576 | tf_op jit(solution)/shard_map/all_to_all | solution.py:42
  69.5 135.0 %copy-start.7 = (bf16[1,2048,256]{2,1,0:T(8,128)(2,1)S(1)}, bf16[1,2048,256]{2,1,0:T(8,128)(2,1)}, u32[]{:S(2)}) copy-start(bf16[1,2048,256]{2,1,0:T(8,128)(2,1)} %param.25) | copy-start | bytes 3145732
  81.7 10.8 %all-to-all-start.2 = ((f32[8,1,128]{2,1,0:T(1,128)}), f32[8,1,128]{2,1,0:T(1,128)S(1)}, u32[]{:S(2)}, u32[]{:S(2)}) async-start(f32[8,1,128]{2,1,0:T(1,128)} %broadcast_in_dim.9), calls=%async_computation.2 | async-start | bytes 8192 | tf_op jit(solution)/shard_map/all_to_all | solution.py:19
  86.0 118.6 %all-gather.2.cloned.1.call-start = ((), (), s32[]{:S(2)}) async-start(), calls=%async_computation.6 | async-start | bytes 4718592 | tf_op jit(solution)/shard_map/all_gather | solution.py:122
  204.5 3.6 copy-start.6
  204.5 3.7 copy-start.8
  309.2 7.5 %copy-start.9 = (bf16[1,2048,256]{2,1,0:T(8,128)(2,1)S(1)}, bf16[1,2048,256]{2,1,0:T(8,128)(2,1)}, u32[]{:S(2)}) copy-start(bf16[1,2048,256]{2,1,0:T(8,128)(2,1)} %param.27) | copy-start | bytes 3145732
  316.7 22.2 %copy-start.3 = (f32[128,4]{0,1:T(4,128)S(1)}, f32[128,4]{0,1:T(4,128)}, u32[]{:S(2)}) copy-start(f32[128,4]{0,1:T(4,128)} %param.24) | copy-start | bytes 6148
  321.0 51.3 %all-to-all-start.5 = ((bf16[32,1,32,256]{3,2,1,0:T(8,128)(2,1)}), bf16[32,1,32,256]{3,2,1,0:T(8,128)(2,1)S(1)}, u32[]{:S(2)}, u32[]{:S(2)}) async-start(bf16[32,1,32,256]{3,2,1,0:T(8,128)(2,1)} %fusion.25), calls=%async_computation.5 | async-start | bytes 1048576 | tf_op jit(solution)/shard_map/all_to_all | solution.py:140
Sparse Core Ops, SparseCore 0:
  150.3 54.2 all-gather.1
